TPU v7x, 512 devices: a whole 4x4x16 slice. The times are simulated.
512 devices in a mesh: tp: 32 (over z, core), dp: 16 (over y, x).
Axes of the slice: x: 4, y: 4, z: 16, core: 2. Of those that a mesh axis runs over, the one named last changes fastest.
Arguments:
- tokens: bfloat16 [256, 4096], P(None, 'dp'), may hold values from -18 to 18
- lengths: int32 [256], P('dp'), may hold values from 1 to 16384, 540672 in all
- gain_one: float32 [4096], P('dp'), may hold values from 0.1 to 1.9
- recept_one: bfloat16 [4096, 2048], P('dp', 'tp'), may hold values from -0.09375 to 0.09375
- key_one: bfloat16 [4096, 2048], P('dp', 'tp'), may hold values from -0.09375 to 0.09375
- value_one: bfloat16 [4096, 2048], P('dp', 'tp'), may hold values from -0.09375 to 0.09375
- decay_one: bfloat16 [4096, 2048], P('dp', 'tp'), may hold values from -0.09375 to 0.09375
- learn_one: bfloat16 [4096, 2048], P('dp', 'tp'), may hold values from -0.09375 to 0.09375
- gate_one: bfloat16 [4096, 2048], P('dp', 'tp'), may hold values from -0.09375 to 0.09375
- pace_one: float32 [16, 2048], P(None, 'tp'), may hold values from -3 to 2
- group_one: float32 [2048], P('tp'), may hold values from 0.1 to 1.9
- output_one: bfloat16 [2048, 4096], P('tp', 'dp'), may hold values from -0.125 to 0.125
- state_one: float32 [256, 32, 4096], P('dp', 'tp'), may hold values from -3 to 3
- gain_two: float32 [4096], P('dp'), may hold values from 0.1 to 1.9
- recept_two: bfloat16 [4096, 2048], P('dp', 'tp'), may hold values from -0.09375 to 0.09375
- key_two: bfloat16 [4096, 2048], P('dp', 'tp'), may hold values from -0.09375 to 0.09375
- value_two: bfloat16 [4096, 2048], P('dp', 'tp'), may hold values from -0.09375 to 0.09375
- decay_two: bfloat16 [4096, 2048], P('dp', 'tp'), may hold values from -0.09375 to 0.09375
- learn_two: bfloat16 [4096, 2048], P('dp', 'tp'), may hold values from -0.09375 to 0.09375
- gate_two: bfloat16 [4096, 2048], P('dp', 'tp'), may hold values from -0.09375 to 0.09375
- pace_two: float32 [16, 2048], P(None, 'tp'), may hold values from -3 to 2
- group_two: float32 [2048], P('tp'), may hold values from 0.1 to 1.9
- output_two: bfloat16 [2048, 4096], P('tp', 'dp'), may hold values from -0.125 to 0.125
- state_two: float32 [256, 32, 4096], P('dp', 'tp'), may hold values from -3 to 3
Outputs:
- mixed: bfloat16 [256, 4096], P(None, 'dp')
- fresh_one: float32 [256, 32, 4096], P('dp', 'tp')
- fresh_two: float32 [256, 32, 4096], P('dp', 'tp')
All inputs are finite; a program needn't handle non-finite values. No bound on the sum of `lengths` on one device may be relied on, other than what follows from the above.
Results may differ from a plain program's by a relative error of at most 0.0069.
Values may be sent and summed in bfloat16 or wider, within the bound.
No kernel may reach another device: no remote copies, remote signals or barrier semaphores. Data moves between devices by JAX's collectives and lax.ppermute only.
A program may use at most 64 MiB of HBM per device.

v0:
```python
import jax
import jax.numpy as jnp
from jax import lax
from jax.sharding import PartitionSpec as P

D = 4096
HEAD = 64
SPAN_LEN = 1024


norm_eps = 1e-06
group_eps = 0.00064


def in_blocks(array, dim, size):
    lengths = array.shape
    parts = array.reshape(*lengths[:dim], size, lengths[dim] // size, *lengths[dim + 1 :])
    return jnp.moveaxis(parts, dim, 0)


def summed_on_arrival(array, axis, dim):
    parts = in_blocks(array, dim, lax.axis_size(axis))
    arrived = lax.all_to_all(parts, axis, split_axis=0, concat_axis=0, tiled=True)
    return arrived.sum(axis=0)


def sent_together(arrays, axis, dim, along):
    columns = [a.reshape(*a.shape[:along], -1) for a in arrays]
    both = jnp.concatenate(columns, axis=along)
    filled, at, gathered = (summed_on_arrival(both, axis, dim), 0, [])
    for a, column in zip(arrays, columns):
        slab = filled[..., at : at + column.shape[along]]
        gathered.append(slab.reshape(*slab.shape[:along], *a.shape[along:]))
        at += column.shape[along]
    return tuple(gathered)


def laid_out(parts, dim):
    parts = jnp.moveaxis(parts, 0, dim)
    lengths = parts.shape
    return parts.reshape(*lengths[:dim], lengths[dim] * lengths[dim + 1], *lengths[dim + 2 :])


def copy_for_each(array, axis):
    copies = jnp.broadcast_to(array, (lax.axis_size(axis), *array.shape))
    return lax.all_to_all(copies, axis, split_axis=0, concat_axis=0, tiled=True)


def collect(array, axis, dim):
    return laid_out(copy_for_each(array, axis), dim)


def recur_block(
    hidden_in, lengths, norm_gain, weights, pace_table, group_gain, output_weight, old_state
):
    floats = hidden_in.astype(jnp.float32)
    seq_count = old_state.shape[0]
    heads_dev = old_state.shape[1]
    squares = jnp.sum(floats * floats, axis=1)
    scaled = (floats * norm_gain).astype(jnp.bfloat16)
    partials = [jnp.dot(scaled, weight, preferred_element_type=jnp.float32) for weight in weights]
    gathered = sent_together(
        (partials[0], partials[1], partials[2], partials[3], partials[4], partials[5], squares),
        "dp",
        0,
        1,
    )
    summed = gathered[:6]
    own_squares = gathered[6]
    inverse = lax.rsqrt(own_squares / D + norm_eps)[:, None]
    span_index = (lengths - 1) // SPAN_LEN
    onehot = (
        span_index[:, None] == jnp.arange(pace_table.shape[0], dtype=jnp.int32)[None, :]
    ).astype(jnp.float32)
    bias_rows = jnp.dot(onehot, pace_table, precision=lax.Precision.HIGHEST)
    recept_rows = inverse * summed[0]
    key_rows = inverse * summed[1]
    value_rows = inverse * summed[2]
    decay_in = inverse * summed[3] + bias_rows
    decay_rate = jnp.exp(-jnp.exp(-jax.nn.softplus(-decay_in) - 0.5))
    learn_rate = jax.nn.sigmoid(inverse * summed[4])
    gate_rows = jax.nn.sigmoid(inverse * summed[5])

    def split_heads(flat_field):
        return flat_field.reshape(seq_count, heads_dev, HEAD)

    recept_rows = split_heads(recept_rows)
    key_rows = split_heads(key_rows)
    value_rows = split_heads(value_rows)
    decay_rate = split_heads(decay_rate)
    learn_rate = split_heads(learn_rate)
    unit_key = key_rows * lax.rsqrt(jnp.sum(key_rows * key_rows, axis=-1, keepdims=True) + 1.0)
    matrix = old_state.reshape(seq_count, heads_dev, HEAD, HEAD)
    removed = jnp.einsum("bhvk,bhk->bhv", matrix, unit_key, precision=lax.Precision.HIGHEST)
    matrix = (
        matrix * decay_rate[:, :, None, :]
        - removed[..., None] * (unit_key * learn_rate)[:, :, None, :]
        + value_rows[..., None] * (key_rows * learn_rate)[:, :, None, :]
    )
    readout = jnp.einsum("bhvk,bhk->bhv", matrix, recept_rows, precision=lax.Precision.HIGHEST)
    center = readout - jnp.mean(readout, axis=-1, keepdims=True)
    normed = center * lax.rsqrt(jnp.mean(center * center, axis=-1, keepdims=True) + group_eps)
    head_mix = (normed.reshape(seq_count, heads_dev * HEAD) * group_gain * gate_rows).astype(
        jnp.bfloat16
    )
    partial_out = jnp.dot(
        collect(head_mix, "dp", 0), output_weight, preferred_element_type=jnp.float32
    )
    col_share = summed_on_arrival(partial_out, "tp", 1)
    share_cols = col_share.shape[1]
    own_cols = lax.dynamic_slice_in_dim(floats, lax.axis_index("tp") * share_cols, share_cols, 1)
    result = collect((own_cols + col_share).astype(jnp.bfloat16), "tp", 1)
    return (result, matrix.reshape(seq_count, heads_dev, HEAD * HEAD))


def body(
    tokens,
    lengths,
    gain_one,
    recept_one,
    key_one,
    value_one,
    decay_one,
    learn_one,
    gate_one,
    pace_one,
    group_one,
    output_one,
    state_one,
    gain_two,
    recept_two,
    key_two,
    value_two,
    decay_two,
    learn_two,
    gate_two,
    pace_two,
    group_two,
    output_two,
    state_two,
):
    middle, fresh_one = recur_block(
        tokens,
        lengths,
        gain_one,
        (recept_one, key_one, value_one, decay_one, learn_one, gate_one),
        pace_one,
        group_one,
        output_one,
        state_one,
    )
    mixed, fresh_two = recur_block(
        middle,
        lengths,
        gain_two,
        (recept_two, key_two, value_two, decay_two, learn_two, gate_two),
        pace_two,
        group_two,
        output_two,
        state_two,
    )
    return (mixed, fresh_one, fresh_two)


def solution(mesh):
    in_specs = (
        P(None, "dp"),
        P("dp"),
        P("dp"),
        P("dp", "tp"),
        P("dp", "tp"),
        P("dp", "tp"),
        P("dp", "tp"),
        P("dp", "tp"),
        P("dp", "tp"),
        P(None, "tp"),
        P("tp"),
        P("tp", "dp"),
        P("dp", "tp", None),
        P("dp"),
        P("dp", "tp"),
        P("dp", "tp"),
        P("dp", "tp"),
        P("dp", "tp"),
        P("dp", "tp"),
        P("dp", "tp"),
        P(None, "tp"),
        P("tp"),
        P("tp", "dp"),
        P("dp", "tp", None),
    )
    out_specs = (P(None, "dp"), P("dp", "tp", None), P("dp", "tp", None))
    return jax.shard_map(body, mesh=mesh, in_specs=in_specs, out_specs=out_specs, check_vma=False)
```

profile of v0, /device:TPU:1, one launch (start us, length us, event | category | flops | bytes accessed | tf_op | source)
XLA Modules:
  0.0 187.1 jit_solution(5632420893200145563)
XLA Ops:
  1.9 1.0 fusion.76
  3.0 1.1 fusion.75
  4.1 1.1 fusion.74
  5.1 1.1 fusion.73
  6.2 1.1 fusion.72
  7.3 1.1 fusion.71
  9.4 7.7 %all-to-all-start = ((f32[16,16,385]{2,1,0:T(8,128)}), f32[16,16,385]{2,1,0:T(8,128)S(1)}, u32[]{:S(2)}, u32[]{:S(2)}) async-start(f32[16,16,385]{2,1,0:T(8,128)} %concatenate.31), calls=%async_computation | async-start | bytes 1048576 | tf_op jit(solution)/shard_map/all_to_all | solution.py:23
  18.0 8.1 %all-to-all-done = f32[16,16,385]{2,1,0:T(8,128)S(1)} async-done(((f32[16,16,385]{2,1,0:T(8,128)}), f32[16,16,385]{2,1,0:T(8,128)S(1)}, u32[]{:S(2)}, u32[]{:S(2)}) %all-to-all-start) | async-done | bytes 394272 | tf_op jit(solution)/shard_map/all_to_all | solution.py:23
  27.8 1.1 fusion.6
  30.1 3.5 %all-to-all-start.1 = ((bf16[16,2,512]{2,1,0:T(2,128)(2,1)}), bf16[16,2,512]{2,1,0:T(2,128)(2,1)S(1)}, u32[]{:S(2)}, u32[]{:S(2)}) async-start(bf16[16,2,512]{2,1,0:T(2,128)(2,1)} %reshape.376), calls=%async_computation.1 | async-start | bytes 65536 | tf_op jit(solution)/shard_map/all_to_all | solution.py:46
  33.7 6.3 %all-to-all-done.1 = bf16[16,2,512]{2,1,0:T(2,128)(2,1)S(1)} async-done(((bf16[16,2,512]{2,1,0:T(2,128)(2,1)}), bf16[16,2,512]{2,1,0:T(2,128)(2,1)S(1)}, u32[]{:S(2)}, u32[]{:S(2)}) %all-to-all-start.1) | async-done | bytes 32800 | tf_op jit(solution)/shard_map/all_to_all | solution.py:46
  41.1 19.8 %all-to-all-start.2 = ((f32[32,256,8]{1,2,0:T(8,128)}), f32[32,256,8]{1,2,0:T(8,128)S(1)}, u32[]{:S(2)}, u32[]{:S(2)}) async-start(f32[32,256,8]{1,2,0:T(8,128)} %copy.110), calls=%async_computation.2 | async-start | bytes 524288 | tf_op jit(solution)/shard_map/all_to_all | solution.py:23
  61.0 22.2 %all-to-all-done.2 = f32[32,256,8]{1,2,0:T(8,128)S(1)} async-done(((f32[32,256,8]{1,2,0:T(8,128)}), f32[32,256,8]{1,2,0:T(8,128)S(1)}, u32[]{:S(2)}, u32[]{:S(2)}) %all-to-all-start.2) | async-done | bytes 262176 | tf_op jit(solution)/shard_map/all_to_all | solution.py:23
  83.3 19.5 %all_to_all.40 = bf16[32,256,8]{1,2,0:T(8,128)(2,1)S(1)} all-to-all(bf16[32,256,8]{1,2,0:T(8,128)(2,1)S(1)} %broadcast_in_dim.9), channel_id=1, replica_groups=mesh['tp'=32,'dp'=16] {'tp'}, dimensions={0} | all-to-all | bytes 262144 | tf_op jit(solution)/shard_map/all_to_all | solution.py:46
  103.6 1.0 copy.112
  106.9 3.7 %all-to-all-start.4 = ((f32[16,16,385]{2,1,0:T(8,128)}), f32[16,16,385]{2,1,0:T(8,128)S(1)}, u32[]{:S(2)}, u32[]{:S(2)}) async-start(f32[16,16,385]{2,1,0:T(8,128)} %concatenate.33), calls=%async_computation.4 | async-start | bytes 1048576 | tf_op jit(solution)/shard_map/all_to_all | solution.py:23
  111.6 9.3 %all-to-all-done.4 = f32[16,16,385]{2,1,0:T(8,128)S(1)} async-done(((f32[16,16,385]{2,1,0:T(8,128)}), f32[16,16,385]{2,1,0:T(8,128)S(1)}, u32[]{:S(2)}, u32[]{:S(2)}) %all-to-all-start.4) | async-done | bytes 394272 | tf_op jit(solution)/shard_map/all_to_all | solution.py:23
  122.6 1.1 fusion.2
  124.9 3.7 %all-to-all-start.5 = ((bf16[16,2,512]{2,1,0:T(2,128)(2,1)}), bf16[16,2,512]{2,1,0:T(2,128)(2,1)S(1)}, u32[]{:S(2)}, u32[]{:S(2)}) async-start(bf16[16,2,512]{2,1,0:T(2,128)(2,1)} %reshape.378), calls=%async_computation.5 | async-start | bytes 65536 | tf_op jit(solution)/shard_map/all_to_all | solution.py:46
  130.0 4.8 %all-to-all-done.5 = bf16[16,2,512]{2,1,0:T(2,128)(2,1)S(1)} async-done(((bf16[16,2,512]{2,1,0:T(2,128)(2,1)}), bf16[16,2,512]{2,1,0:T(2,128)(2,1)S(1)}, u32[]{:S(2)}, u32[]{:S(2)}) %all-to-all-start.5) | async-done | bytes 32800 | tf_op jit(solution)/shard_map/all_to_all | solution.py:46
  136.0 6.8 %all-to-all-start.6 = ((f32[32,256,8]{1,2,0:T(8,128)}), f32[32,256,8]{1,2,0:T(8,128)S(1)}, u32[]{:S(2)}, u32[]{:S(2)}) async-start(f32[32,256,8]{1,2,0:T(8,128)} %copy.117), calls=%async_computation.6 | async-start | bytes 524288 | tf_op jit(solution)/shard_map/all_to_all | solution.py:23
  144.9 19.5 %all-to-all-done.6 = f32[32,256,8]{1,2,0:T(8,128)S(1)} async-done(((f32[32,256,8]{1,2,0:T(8,128)}), f32[32,256,8]{1,2,0:T(8,128)S(1)}, u32[]{:S(2)}, u32[]{:S(2)}) %all-to-all-start.6) | async-done | bytes 262176 | tf_op jit(solution)/shard_map/all_to_all | solution.py:23
  165.1 5.0 %all-to-all-start.7 = ((bf16[32,256,8]{1,2,0:T(8,128)(2,1)}), bf16[32,256,8]{1,2,0:T(8,128)(2,1)S(1)}, u32[]{:S(2)}, u32[]{:S(2)}) async-start(bf16[32,256,8]{1,2,0:T(8,128)(2,1)} %broadcast_in_dim.11), calls=%async_computation.7 | async-start | bytes 262144 | tf_op jit(solution)/shard_map/all_to_all | solution.py:46
  170.9 15.4 %all-to-all-done.7 = bf16[32,256,8]{1,2,0:T(8,128)(2,1)S(1)} async-done(((bf16[32,256,8]{1,2,0:T(8,128)(2,1)}), bf16[32,256,8]{1,2,0:T(8,128)(2,1)S(1)}, u32[]{:S(2)}, u32[]{:S(2)}) %all-to-all-start.7) | async-done | bytes 131104 | tf_op jit(solution)/shard_map/all_to_all | solution.py:46
  (111 shorter events, 20.6 us)
Async XLA Ops:
  0.6 1.3 copy-start
  1.9 15.2 %copy-start.1 = (f32[16,1,4096]{2,1,0:T(1,128)S(1)}, f32[16,1,4096]{2,1,0:T(1,128)}, u32[]{:S(2)}) copy-start(f32[16,1,4096]{2,1,0:T(1,128)} %param.36) | copy-start | bytes 786436
  7.3 10.7 %copy-start.16 = (s32[16]{0:T(128)S(1)}, s32[16]{0:T(128)}, u32[]{:S(2)}) copy-start(s32[16]{0:T(128)} %param.25) | copy-start | bytes 196
  9.4 18.1 %copy-start.14 = (f32[16,64]{1,0:T(8,128)S(1)}, f32[16,64]{1,0:T(8,128)}, u32[]{:S(2)}) copy-start(f32[16,64]{1,0:T(8,128)} %param.33) | copy-start | bytes 12292
  9.4 19.8 %copy-start.12 = (f32[64]{0:T(128)S(1)}, f32[64]{0:T(128)}, u32[]{:S(2)}) copy-start(f32[64]{0:T(128)} %param.34) | copy-start | bytes 772
  9.4 16.8 %all-to-all-start = ((f32[16,16,385]{2,1,0:T(8,128)}), f32[16,16,385]{2,1,0:T(8,128)S(1)}, u32[]{:S(2)}, u32[]{:S(2)}) async-start(f32[16,16,385]{2,1,0:T(8,128)} %concatenate.31), calls=%async_computation | async-start | bytes 1048576 | tf_op jit(solution)/shard_map/all_to_all | solution.py:23
  17.1 16.5 %copy-start.3 = (bf16[64,256]{1,0:T(8,128)(2,1)S(1)}, bf16[64,256]{1,0:T(8,128)(2,1)}, u32[]{:S(2)}) copy-start(bf16[64,256]{1,0:T(8,128)(2,1)} %param.35) | copy-start | bytes 98308
  30.1 9.9 %all-to-all-start.1 = ((bf16[16,2,512]{2,1,0:T(2,128)(2,1)}), bf16[16,2,512]{2,1,0:T(2,128)(2,1)S(1)}, u32[]{:S(2)}, u32[]{:S(2)}) async-start(bf16[16,2,512]{2,1,0:T(2,128)(2,1)} %reshape.376), calls=%async_computation.1 | async-start | bytes 65536 | tf_op jit(solution)/shard_map/all_to_all | solution.py:46
  41.1 42.1 %all-to-all-start.2 = ((f32[32,256,8]{1,2,0:T(8,128)}), f32[32,256,8]{1,2,0:T(8,128)S(1)}, u32[]{:S(2)}, u32[]{:S(2)}) async-start(f32[32,256,8]{1,2,0:T(8,128)} %copy.110), calls=%async_computation.2 | async-start | bytes 524288 | tf_op jit(solution)/shard_map/all_to_all | solution.py:23
  102.8 1.7 copy-start.11
  102.9 1.8 copy-start.4
  103.5 1.3 copy-start.5
  103.5 1.5 copy-start.6
  103.5 1.6 copy-start.7
  103.5 1.8 copy-start.8
  103.6 1.9 %copy-start.9 = (bf16[256,64]{0,1:T(8,128)(2,1)S(1)}, bf16[256,64]{0,1:T(8,128)(2,1)}, u32[]{:S(2)}) copy-start(bf16[256,64]{0,1:T(8,128)(2,1)} %param.38) | copy-start | bytes 98308
  104.8 5.9 %copy-start.2 = (f32[16,1,4096]{2,1,0:T(1,128)S(1)}, f32[16,1,4096]{2,1,0:T(1,128)}, u32[]{:S(2)}) copy-start(f32[16,1,4096]{2,1,0:T(1,128)} %param.47) | copy-start | bytes 786436
  105.7 5.8 %copy-start.10 = (bf16[64,256]{1,0:T(8,128)(2,1)S(1)}, bf16[64,256]{1,0:T(8,128)(2,1)}, u32[]{:S(2)}) copy-start(bf16[64,256]{1,0:T(8,128)(2,1)} %param.46) | copy-start | bytes 98308
  106.0 15.5 %copy-start.15 = (f32[16,64]{1,0:T(8,128)S(1)}, f32[16,64]{1,0:T(8,128)}, u32[]{:S(2)}) copy-start(f32[16,64]{1,0:T(8,128)} %param.44) | copy-start | bytes 12292
  106.9 17.1 %copy-start.13 = (f32[64]{0:T(128)S(1)}, f32[64]{0:T(128)}, u32[]{:S(2)}) copy-start(f32[64]{0:T(128)} %param.45) | copy-start | bytes 772
  106.9 14.0 %all-to-all-start.4 = ((f32[16,16,385]{2,1,0:T(8,128)}), f32[16,16,385]{2,1,0:T(8,128)S(1)}, u32[]{:S(2)}, u32[]{:S(2)}) async-start(f32[16,16,385]{2,1,0:T(8,128)} %concatenate.33), calls=%async_computation.4 | async-start | bytes 1048576 | tf_op jit(solution)/shard_map/all_to_all | solution.py:23
  124.9 9.9 %all-to-all-start.5 = ((bf16[16,2,512]{2,1,0:T(2,128)(2,1)}), bf16[16,2,512]{2,1,0:T(2,128)(2,1)S(1)}, u32[]{:S(2)}, u32[]{:S(2)}) async-start(bf16[16,2,512]{2,1,0:T(2,128)(2,1)} %reshape.378), calls=%async_computation.5 | async-start | bytes 65536 | tf_op jit(solution)/shard_map/all_to_all | solution.py:46
  136.0 28.5 %all-to-all-start.6 = ((f32[32,256,8]{1,2,0:T(8,128)}), f32[32,256,8]{1,2,0:T(8,128)S(1)}, u32[]{:S(2)}, u32[]{:S(2)}) async-start(f32[32,256,8]{1,2,0:T(8,128)} %copy.117), calls=%async_computation.6 | async-start | bytes 524288 | tf_op jit(solution)/shard_map/all_to_all | solution.py:23
  165.1 21.2 %all-to-all-start.7 = ((bf16[32,256,8]{1,2,0:T(8,128)(2,1)}), bf16[32,256,8]{1,2,0:T(8,128)(2,1)S(1)}, u32[]{:S(2)}, u32[]{:S(2)}) async-start(bf16[32,256,8]{1,2,0:T(8,128)(2,1)} %broadcast_in_dim.11), calls=%async_computation.7 | async-start | bytes 262144 | tf_op jit(solution)/shard_map/all_to_all | solution.py:46
where the time goes:
time: 188 us; the launch traced here: 187 us
  waiting for transfers between devices  85.8 us (46%)
  starting transfers between devices  50.2 us (27%)
  blocking collectives  19.5 us (10%)
  local copies, waits for them, and re-layouts  12.6 us (7%)
  matrix products  12.3 us (7%)
  other arithmetic  5.36 us (3%)
    all_to_all x4, waiting for transfers between devices, summed_on_arrival(): lax.all_to_all(parts, axis, split_axis=0, concat_axis=0, tiled=True)  59.2 us
    all_to_all x4, starting transfers between devices, summed_on_arrival(): lax.all_to_all(parts, axis, split_axis=0, concat_axis=0, tiled=True)  38.1 us
    all_to_all x3, waiting for transfers between devices, copy_for_each(): return lax.all_to_all(copies, axis, split_axis=0, concat_axis=0, tiled=True)  26.5 us
    all_to_all x1, blocking collectives, copy_for_each(): return lax.all_to_all(copies, axis, split_axis=0, concat_axis=0, tiled=True)  19.5 us
    all_to_all x3, starting transfers between devices, copy_for_each(): return lax.all_to_all(copies, axis, split_axis=0, concat_axis=0, tiled=True)  12.2 us
    dot_general x12, matrix products, recur_block(): jnp.dot(scaled, weight, preferred_element_type=jnp.float32)  7.34 us
    unnamed x42, local copies, waits for them, and re-layouts  3.77 us
  transfers between devices with their start and end apart: 7, of which 7 were waited for; matrix products, arithmetic and copies ran while one was open for 3% of the time, Pallas kernels for 0%

commit v1 on v0

v1 whole, which is shorter than its diff:
```python
import functools

import jax
import jax.numpy as jnp
from jax import lax
from jax.experimental import pallas as pl
from jax.experimental.pallas import tpu as pltpu
from jax.sharding import PartitionSpec as P

D = 4096
HEAD = 64
SPAN_SHIFT = 10
LANES = 128
norm_eps = 1e-06
group_eps = 0.00064
half_decay = 0.6065306597126334

f32 = jnp.float32
bf16 = jnp.bfloat16


def exchange(parts, axis):
    return lax.all_to_all(parts, axis, split_axis=0, concat_axis=0, tiled=True)


def dot_last(left, right):
    return lax.dot_general(left, right, (((1,), (1,)), ((), ())), preferred_element_type=f32)


def exact_dot(left, right):
    return jnp.dot(left, right, precision=lax.Precision.HIGHEST, preferred_element_type=f32)


def twice(rows):
    return jnp.concatenate([rows, rows], axis=1)


def sigmoid(values):
    return 1.0 / (1.0 + jnp.exp(-values))


def state_step(first, second, third, inverse, lengths, pace_ref, group, state):
    seqs = first.shape[0]
    tiles = state.shape[0] // seqs
    first, second, third = first * inverse, second * inverse, third * inverse
    recept, key = first[:, :HEAD], first[:, HEAD:]
    value, decay_in = second[:, :HEAD], second[:, HEAD:]
    learn_in, gate_in = third[:, :HEAD], third[:, HEAD:]
    span = (lengths - 1) >> SPAN_SHIFT
    for s in range(pace_ref.shape[0]):
        decay_in = decay_in + jnp.where(span == s, pace_ref[s : s + 1, :], 0.0)
    decay_rate = jnp.exp(-half_decay * sigmoid(decay_in))
    learn_rate = sigmoid(learn_in)
    gate_rows = sigmoid(gate_in)
    unit_key = key * lax.rsqrt(jnp.sum(key * key, axis=1, keepdims=True) + 1.0)

    lane = lax.broadcasted_iota(jnp.int32, (LANES, LANES), 0) // HEAD
    column = lax.broadcasted_iota(jnp.int32, (LANES, LANES), 1) // HEAD
    same_half = (lane == column).astype(f32)
    lane = lax.broadcasted_iota(jnp.int32, (LANES, HEAD), 0) // HEAD
    column = lax.broadcasted_iota(jnp.int32, (LANES, HEAD), 1) & 1
    to_values = (lane == column).astype(f32)
    lane = lax.broadcasted_iota(jnp.int32, (HEAD, LANES), 0) & 1
    column = lax.broadcasted_iota(jnp.int32, (HEAD, LANES), 1) // HEAD
    from_values = (lane == column).astype(f32)
    tile = lax.broadcasted_iota(jnp.int32, (seqs, tiles, HEAD), 1)
    own_tile = tile == (lax.broadcasted_iota(jnp.int32, (seqs, tiles, HEAD), 2) >> 1)

    def flat(cube):
        return cube.reshape(seqs * tiles, cube.shape[2])

    def cubed(rows):
        return rows.reshape(seqs, tiles, rows.shape[1])

    matrix = cubed(state)
    removed = cubed(exact_dot(flat(matrix * twice(unit_key)[:, None, :]), same_half))
    spread = jnp.where(own_tile, jnp.broadcast_to(value[:, None, :], own_tile.shape), 0.0)
    values = cubed(exact_dot(flat(spread), from_values))
    fresh = (
        matrix * twice(decay_rate)[:, None, :]
        - removed * twice(unit_key * learn_rate)[:, None, :]
        + values * twice(key * learn_rate)[:, None, :]
    )
    read = cubed(exact_dot(flat(fresh * twice(recept)[:, None, :]), to_values))
    readout = jnp.sum(jnp.where(own_tile, read, 0.0), axis=1)
    center = readout - jnp.mean(readout, axis=1, keepdims=True)
    normed = center * lax.rsqrt(jnp.mean(center * center, axis=1, keepdims=True) + group_eps)
    head_mix = (normed * group * gate_rows).astype(bf16)
    return head_mix, flat(fresh)


def pack_kernel(*refs):
    weights, output, gain, packed = refs[:6], refs[6], refs[7], refs[8]
    for i, weight in enumerate(weights):
        packed[HEAD * i : HEAD * (i + 1), :] = weight[...]
    packed[6 * HEAD : 7 * HEAD, :] = output[...]
    values = gain[...]
    high = values.astype(bf16).astype(f32)
    middle = (values - high).astype(bf16).astype(f32)
    low = values - high - middle
    row = lax.broadcasted_iota(jnp.int32, (16, values.shape[1]), 0)
    parts = jnp.where(row == 0, high, jnp.where(row == 1, middle, jnp.where(row == 2, low, 0.0)))
    packed[7 * HEAD :, :] = parts.astype(bf16)


def project_kernel(*refs):
    tokens, gain, weights, output, parts = refs[0], refs[1], refs[2:8], refs[8], refs[9]
    groups = parts.shape[0]
    rows = tokens.shape[0] // groups
    scaled = (tokens[...].astype(f32) * gain[...]).astype(bf16)
    for i in range(3):
        pair = jnp.concatenate([weights[2 * i][...], weights[2 * i + 1][...]], axis=0)
        product = dot_last(scaled, pair).astype(bf16)
        parts[:, rows * i : rows * (i + 1), :] = product.reshape(groups, rows, LANES)
    for h in range(2):
        columns = slice(LANES * h, LANES * (h + 1))
        start = rows * (3 + h)
        parts[:, start : start + rows, :] = tokens[:, columns].reshape(groups, rows, LANES)
        start = 5 * rows + HEAD * h
        parts[:, start : start + HEAD, :] = jnp.broadcast_to(
            output[:, columns][None], (groups, HEAD, LANES)
        )


def first_step_kernel(arrived, lengths, pace, group, state, parts, fresh):
    groups = arrived.shape[0]
    rows = parts.shape[1]
    sums = [
        jnp.sum(arrived[:, rows * i : rows * (i + 1), :].astype(f32), axis=0) for i in range(3)
    ]
    token_rows = arrived[:, 3 * rows : 4 * rows, :].astype(f32)
    other_rows = arrived[:, 4 * rows : 5 * rows, :].astype(f32)
    squares = jnp.sum(token_rows * token_rows + other_rows * other_rows, axis=0)
    squares = jnp.sum(squares, axis=1, keepdims=True)
    inverse = lax.rsqrt(squares / D + norm_eps)
    head_mix, new_state = state_step(
        *sums, inverse, lengths[...], pace, group[...], state[...]
    )
    for d in range(groups):
        for h in range(2):
            start = 5 * rows + HEAD * h
            product = jnp.dot(
                head_mix, arrived[d, start : start + HEAD, :], preferred_element_type=f32
            )
            parts[2 * d + h] = product.astype(bf16)
    fresh[...] = new_state


def second_step_kernel(
    middle, gathered, lengths, pace, group, state, parts, fresh, held, arrivals
):
    groups = held.shape[0]
    copies = [
        pltpu.make_async_copy(gathered.at[d], held.at[d], arrivals.at[d]) for d in range(groups)
    ]
    for copy in copies:
        copy.start()
    floats = middle[...].astype(f32)
    squares = jnp.sum(jnp.sum(floats * floats, axis=0), axis=1, keepdims=True)
    inverse = lax.rsqrt(squares / D + norm_eps)
    sums = jnp.zeros((floats.shape[1], 6 * HEAD), f32)
    for d in range(groups):
        copies[d].wait()
        gains = held[d, 7 * HEAD :, :].astype(f32)
        gain = gains[0:1] + gains[1:2] + gains[2:3]
        columns = jnp.concatenate([floats[2 * d], floats[2 * d + 1]], axis=1)
        scaled = (columns * gain).astype(bf16)
        sums = sums + dot_last(scaled, held[d, : 6 * HEAD, :])
    head_mix, new_state = state_step(
        sums[:, :LANES],
        sums[:, LANES : 2 * LANES],
        sums[:, 2 * LANES :],
        inverse,
        lengths[...],
        pace,
        group[...],
        state[...],
    )
    for d in range(groups):
        product = jnp.dot(
            head_mix, held[d, 6 * HEAD : 7 * HEAD, :], preferred_element_type=f32
        ).astype(bf16)
        parts[2 * d] = product[:, :LANES]
        parts[2 * d + 1] = product[:, LANES:]
    fresh[...] = new_state


def add_kernel(shares, own, copies, result):
    total = own[...].astype(f32) + jnp.sum(shares[...].astype(f32), axis=0)
    rounded = total.astype(bf16)
    result[...] = rounded
    copies[...] = jnp.broadcast_to(rounded[None], copies.shape)


def call(kernel, name, out_shape, *args, **options):
    return pl.pallas_call(kernel, name=name, out_shape=out_shape, **options)(*args)


def shape(*lengths, dtype=bf16):
    return jax.ShapeDtypeStruct(lengths, dtype)


def body(
    tokens,
    lengths,
    gain_one,
    recept_one,
    key_one,
    value_one,
    decay_one,
    learn_one,
    gate_one,
    pace_one,
    group_one,
    output_one,
    state_one,
    gain_two,
    recept_two,
    key_two,
    value_two,
    decay_two,
    learn_two,
    gate_two,
    pace_two,
    group_two,
    output_two,
    state_two,
):
    dp, tp = lax.axis_size("dp"), lax.axis_size("tp")
    rows, cols = tokens.shape
    seqs = rows // dp
    state_rows = seqs * HEAD * HEAD // LANES
    weights_one = [w.T for w in (recept_one, key_one, value_one, decay_one, learn_one, gate_one)]
    weights_two = [w.T for w in (recept_two, key_two, value_two, decay_two, learn_two, gate_two)]
    depth = 7 * HEAD + 16
    packed = call(
        pack_kernel, "pack", shape(depth, cols), *weights_two, output_two, gain_two[None]
    )
    gathered = lax.all_gather(packed, "dp")
    lengths = lengths[:, None]

    parts = call(
        project_kernel,
        "project",
        shape(dp, 5 * seqs + 2 * HEAD, LANES),
        tokens,
        gain_one[None],
        *weights_one,
        output_one,
    )
    arrived = exchange(parts, "dp")
    parts, fresh_one = call(
        first_step_kernel,
        "first_step",
        (shape(tp, seqs, LANES), shape(state_rows, LANES, dtype=f32)),
        arrived,
        lengths,
        pace_one,
        group_one[None],
        state_one.reshape(state_rows, LANES),
    )
    own = lax.axis_index("tp")
    own_tokens = lax.dynamic_slice(
        arrived, (own // 2, seqs * (3 + own % 2), 0), (1, seqs, LANES)
    )[0]
    both = (shape(tp, seqs, LANES), shape(seqs, LANES))
    copies, middle_own = call(add_kernel, "add_one", both, exchange(parts, "tp"), own_tokens)
    middle = exchange(copies, "tp")

    whole = functools.partial(pl.BlockSpec, memory_space=pltpu.VMEM)
    parts, fresh_two = call(
        second_step_kernel,
        "second_step",
        (shape(tp, seqs, LANES), shape(state_rows, LANES, dtype=f32)),
        middle,
        gathered,
        lengths,
        pace_two,
        group_two[None],
        state_two.reshape(state_rows, LANES),
        in_specs=[whole(), pl.BlockSpec(memory_space=pl.ANY), whole(), whole(), whole(), whole()],
        scratch_shapes=[pltpu.VMEM((dp, depth, cols), bf16), pltpu.SemaphoreType.DMA((dp,))],
    )
    copies, _ = call(add_kernel, "add_two", both, exchange(parts, "tp"), middle_own)
    mixed = exchange(exchange(copies, "tp"), "dp")
    mixed = mixed.reshape(dp, 2, seqs, LANES).transpose(0, 2, 1, 3).reshape(rows, cols)
    return mixed, fresh_one.reshape(seqs, 1, -1), fresh_two.reshape(seqs, 1, -1)


def solution(mesh):
    weight_specs = (P("dp", "tp"),) * 6
    block_specs = (
        P("dp"),
        *weight_specs,
        P(None, "tp"),
        P("tp"),
        P("tp", "dp"),
        P("dp", "tp", None),
    )
    in_specs = (P(None, "dp"), P("dp"), *block_specs, *block_specs)
    out_specs = (P(None, "dp"), P("dp", "tp", None), P("dp", "tp", None))
    return jax.shard_map(body, mesh=mesh, in_specs=in_specs, out_specs=out_specs, check_vma=False)
```

time: 188 us -> 163 us (0.87)
  waiting for transfers between devices: 85.8 us -> 25.6 us
  blocking collectives: 19.5 us -> 74.1 us
  starting transfers between devices: 50.2 us -> 26.8 us
  Pallas kernels: 0 us -> 17.1 us
  between operations: 1.38 us -> 14.1 us
  matrix products: 12.3 us -> 0 us
  local copies, waits for them, and re-layouts: 12.6 us -> 4.97 us
  other arithmetic: 5.36 us -> 0 us
    all_to_all x7 -> x2, waiting for transfers between devices: 85.8 us -> 25.6 us  [exchange(): return lax.all_to_all(parts, axis, split_axis=0, concat_axis=0, tiled=True)]
    all_to_all x1 -> x4, blocking collectives: 19.5 us -> 74.1 us  [exchange(): return lax.all_to_all(parts, axis, split_axis=0, concat_axis=0, tiled=True)]
    all_to_all x7 -> x2, starting transfers between devices: 50.2 us -> 26.7 us  [exchange(): return lax.all_to_all(parts, axis, split_axis=0, concat_axis=0, tiled=True)]
    pallas_call x0 -> x6, Pallas kernels: none -> 17.1 us  [call(): pl.pallas_call(kernel, name=name, out_shape=out_shape, **options)(*args)]
    dot_general x20 -> x0, matrix products: 12.3 us -> none  [the longest x12 7.34 us: recur_block(): jnp.dot(scaled, weight, preferred_element_type=jnp.float32)]
    concatenate x4 -> x0, local copies, waits for them, and re-layouts: 2.35 us -> none  [sent_together(): both = jnp.concatenate(columns, axis=along)]
    mul x8 -> x0, local copies, waits for them, and re-layouts: 2 us -> none  [the longest x4 0.72 us: recur_block(): matrix * decay_rate[:, :, None, :]]
    unnamed x42 -> x5, local copies, waits for them, and re-layouts: 3.77 us -> 2.26 us
  transfers between devices with their start and end apart: 7 -> 3, of which waited for: 7 -> 2; matrix products, arithmetic and copies ran while one was open for 3% -> 2% of each run, Pallas kernels for 0% -> 5%
where the time goes in v1:
time: 163 us
  blocking collectives  74.1 us (45%)
  starting transfers between devices  26.8 us (16%)
  waiting for transfers between devices  25.6 us (16%)
  Pallas kernels  17.1 us (10%)
  between operations  14.1 us (9%)
  local copies, waits for them, and re-layouts  4.97 us (3%)
    all_to_all x4, blocking collectives, exchange(): return lax.all_to_all(parts, axis, split_axis=0, concat_axis=0, tiled=True)  74.1 us
    all_to_all x2, starting transfers between devices, exchange(): return lax.all_to_all(parts, axis, split_axis=0, concat_axis=0, tiled=True)  26.7 us
    all_to_all x2, waiting for transfers between devices, exchange(): return lax.all_to_all(parts, axis, split_axis=0, concat_axis=0, tiled=True)  25.6 us
    pallas_call x6, Pallas kernels, call(): pl.pallas_call(kernel, name=name, out_shape=out_shape, **options)(*args)  17.1 us
  transfers between devices with their start and end apart: 3, of which 2 were waited for; matrix products, arithmetic and copies ran while one was open for 2% of the time, Pallas kernels for 5%

profile of v1, /device:TPU:1, one launch (start us, length us, event | category | flops | bytes accessed | tf_op | source)
XLA Modules:
  0.0 162.6 jit_solution(3110177654895762260)
XLA Ops:
  7.2 0.0 all-gather.3.cloned.1.call-start
  7.2 1.6 pack.1
  8.8 0.0 all-gather.3.cloned.1.call-update
  8.8 2.2 %project.1 = bf16[16,208,128]{2,1,0:T(8,128)(2,1)} custom-call(bf16[256,256]{1,0:T(8,128)(2,1)} %refs_0_.1, f32[1,256]{1,0:T(1,128)} %bitcast.51, bf16[64,256]{1,0:T(8,128)(2,1)} %bitcast.44, bf16[64,256]{1,0:T(8,128)(2,1)} %bitcast.45, bf16[64,256]{1,0:T(8,128)(2,1)} %bitcast.46, bf16[64,256]{1,0:T(8,128)(2,1)} %bitcast.47, bf16[64,256]{1,0:T(8,128)(2,1)} %bitcast.48, ...), custom_call_target="tpu_custom_call" | custom-call | tf_op jit(solution)/shard_map/project/pallas_call | solution.py:196
  11.0 7.6 %all-to-all-start = ((bf16[16,208,128]{2,1,0:T(8,128)(2,1)}), bf16[16,208,128]{2,1,0:T(8,128)(2,1)S(1)}, u32[]{:S(2)}, u32[]{:S(2)}) async-start(bf16[16,208,128]{2,1,0:T(8,128)(2,1)} %project.1), calls=%async_computation | async-start | bytes 1703936 | tf_op jit(solution)/shard_map/all_to_all | solution.py:23
  18.6 1.3 copy.27.lengths
  19.9 11.0 %all-to-all-done.arrived = bf16[16,208,128]{2,1,0:T(8,128)(2,1)S(1)} async-done(((bf16[16,208,128]{2,1,0:T(8,128)(2,1)}), bf16[16,208,128]{2,1,0:T(8,128)(2,1)S(1)}, u32[]{:S(2)}, u32[]{:S(2)}) %all-to-all-start) | async-done | bytes 852000 | tf_op jit(solution)/shard_map/all_to_all | solution.py:23
  30.9 0.0 copy-start
  31.0 0.9 copy-done
  31.9 3.8 %first_step.1 = (bf16[32,16,128]{2,1,0:T(8,128)(2,1)}, f32[512,128]{1,0:T(8,128)}) custom-call(bf16[16,208,128]{2,1,0:T(8,128)(2,1)} %copy-done, s32[16,1]{1,0:T(8,128)} %copy.27.lengths, f32[16,64]{1,0:T(8,128)} %pace.2, f32[1,64]{1,0:T(1,128)} %bitcast.52, f32[512,128]{1,0:T(8,128)} %bitcast.36), custom_call_target="tpu_custom_call" | custom-call | tf_op jit(solution)/shard_map/first_step/pallas_call | solution.py:196
  35.7 19.2 %all-to-all-start.1 = ((bf16[32,16,128]{2,1,0:T(8,128)(2,1)}), bf16[32,16,128]{2,1,0:T(8,128)(2,1)S(1)}, u32[]{:S(2)}, u32[]{:S(2)}) async-start(bf16[32,16,128]{2,1,0:T(8,128)(2,1)} %get-tuple-element.10), calls=%async_computation.1 | async-start | bytes 262144 | tf_op jit(solution)/shard_map/all_to_all | solution.py:23
  54.9 1.3 dynamic-slice_bitcast_fusion.own
  56.1 14.5 %all-to-all-done.1.shares = bf16[32,16,128]{2,1,0:T(8,128)(2,1)S(1)} async-done(((bf16[32,16,128]{2,1,0:T(8,128)(2,1)}), bf16[32,16,128]{2,1,0:T(8,128)(2,1)S(1)}, u32[]{:S(2)}, u32[]{:S(2)}) %all-to-all-start.1) | async-done | bytes 131104 | tf_op jit(solution)/shard_map/all_to_all | solution.py:23
  70.7 0.0 copy-start.1
  70.7 0.7 copy-done.1
  71.3 1.6 %add_one.1 = (bf16[32,16,128]{2,1,0:T(8,128)(2,1)}, bf16[16,128]{1,0:T(8,128)(2,1)}) custom-call(bf16[32,16,128]{2,1,0:T(8,128)(2,1)} %copy-done.1, bf16[16,128]{1,0:T(8,128)(2,1)} %dynamic-slice_bitcast_fusion.own), custom_call_target="tpu_custom_call" | custom-call | tf_op jit(solution)/shard_map/add_one/pallas_call | solution.py:196
  73.0 22.0 %all_to_all.30.middle = bf16[32,16,128]{2,1,0:T(8,128)(2,1)} all-to-all(bf16[32,16,128]{2,1,0:T(8,128)(2,1)} %get-tuple-element.11), channel_id=1, replica_groups=mesh['tp'=32,'dp'=16] {'tp'}, dimensions={0} | all-to-all | bytes 262144 | tf_op jit(solution)/shard_map/all_to_all | solution.py:23
  94.9 6.2 %second_step.1 = (bf16[32,16,128]{2,1,0:T(8,128)(2,1)}, f32[512,128]{1,0:T(8,128)}) custom-call(bf16[32,16,128]{2,1,0:T(8,128)(2,1)} %all_to_all.30.middle, bf16[16,464,256]{2,1,0:T(8,128)(2,1)} %bitcast.32, s32[16,1]{1,0:T(8,128)} %copy.27.lengths, f32[16,64]{1,0:T(8,128)} %pace.3, f32[1,64]{1,0:T(1,128)} %bitcast.53, f32[512,128]{1,0:T(8,128)} %bitcast.35), custom_call_target="tpu_custom_call" | custom-call | tf_op jit(solution)/shard_map/second_step/pallas_call | solution.py:196
  101.2 21.7 %all_to_all.31.shares = bf16[32,16,128]{2,1,0:T(8,128)(2,1)} all-to-all(bf16[32,16,128]{2,1,0:T(8,128)(2,1)} %get-tuple-element.12), channel_id=1, replica_groups=mesh['tp'=32,'dp'=16] {'tp'}, dimensions={0} | all-to-all | bytes 262144 | tf_op jit(solution)/shard_map/all_to_all | solution.py:23
  122.9 1.6 add_two.1
  124.5 21.0 %all_to_all.32 = bf16[32,16,128]{2,1,0:T(8,128)(2,1)S(1)} all-to-all(bf16[32,16,128]{2,1,0:T(8,128)(2,1)} %get-tuple-element.14), channel_id=1, replica_groups=mesh['tp'=32,'dp'=16] {'tp'}, dimensions={0} | all-to-all | bytes 262144 | tf_op jit(solution)/shard_map/all_to_all | solution.py:23
  145.5 9.4 %all_to_all.33 = bf16[32,16,128]{2,1,0:T(8,128)(2,1)S(1)} all-to-all(bf16[32,16,128]{2,1,0:T(8,128)(2,1)S(1)} %all_to_all.32), channel_id=1, replica_groups=mesh['tp'=32,'dp'=16] {'dp'}, dimensions={0} | all-to-all | bytes 262144 | tf_op jit(solution)/shard_map/all_to_all | solution.py:23
  155.0 0.1 copy.29
  155.1 0.7 copy.34
  (1 shorter events, 0.0 us)
Async XLA Ops:
  7.2 87.8 %all-gather.3.cloned.1.call-start = ((), (), s32[]{:S(2)}) async-start(), calls=%async_computation.6 | async-start | bytes 4038656 | tf_op jit(solution)/shard_map/all_gather | solution.py:239
  11.0 19.9 %all-to-all-start = ((bf16[16,208,128]{2,1,0:T(8,128)(2,1)}), bf16[16,208,128]{2,1,0:T(8,128)(2,1)S(1)}, u32[]{:S(2)}, u32[]{:S(2)}) async-start(bf16[16,208,128]{2,1,0:T(8,128)(2,1)} %project.1), calls=%async_computation | async-start | bytes 1703936 | tf_op jit(solution)/shard_map/all_to_all | solution.py:23
  30.9 0.9 copy-start
  35.7 35.0 %all-to-all-start.1 = ((bf16[32,16,128]{2,1,0:T(8,128)(2,1)}), bf16[32,16,128]{2,1,0:T(8,128)(2,1)S(1)}, u32[]{:S(2)}, u32[]{:S(2)}) async-start(bf16[32,16,128]{2,1,0:T(8,128)(2,1)} %get-tuple-element.10), calls=%async_computation.1 | async-start | bytes 262144 | tf_op jit(solution)/shard_map/all_to_all | solution.py:23
  70.7 0.7 copy-start.1
Sparse Core Ops, SparseCore 0:
  11.6 70.0 all-gather.2
